TPU v7x, 32 devices: a whole 2x2x4 slice. The times are simulated.
32 devices in a mesh: sp: 8 (over z, x), tp: 4 (over y, core).
Axes of the slice: x: 2, y: 2, z: 4, core: 2. Of those that a mesh axis runs over, the one named last changes fastest.
Arguments:
- tokens: bfloat16 [1024, 1024], P('sp', 'tp'), may hold values from -6 to 6
- norm_gain: float32 [3, 1024], replicated, may hold values from 0.1 to 1.9
- w_query: bfloat16 [3, 1024, 1024], P(None, 'sp', 'tp'), may hold values from -0.1875 to 0.1875
- w_key: bfloat16 [3, 1024, 1024], P(None, 'sp', 'tp'), may hold values from -0.1875 to 0.1875
- w_value: bfloat16 [3, 1024, 1024], P(None, 'sp', 'tp'), may hold values from -0.1875 to 0.1875
- w_out: bfloat16 [3, 1024, 1024], P(None, 'tp', 'sp'), may hold values from -0.5625 to 0.5625
- offset_bias: float32 [3, 16, 8, 16], P(None, 'tp'), may hold values from -3 to 3
- documents: int32 [1024], P('sp'), may hold values from 0 to 7, never falling along the last dimension, each value on 1 to 256 neighbouring positions
Outputs:
- mixed: bfloat16 [1024, 1024], P('sp', 'tp')
Inputs may be any that keep to these rules, and one draw needn't show every extreme that they name: `documents`: document numbers never fall along the token order, start at 0, and each document has 1 to 256 tokens.
All inputs are finite; a program needn't handle non-finite values.
Results may differ from a plain program's by a relative error of at most 0.02.
Values may be sent and summed in bfloat16 or wider, within the bound.
A program may use at most 64 MiB of HBM per device.

v0:
```python
import jax
import jax.numpy as jnp
from jax import lax
from jax.sharding import PartitionSpec as P

HEAD_DIM = 64
WIN_ROWS = 8
WIN_COLS = 16
LAYERS = 3
GRID_W = 32
EPS = 1e-06


def with_halo(shard, sides, width, wrap):
    for axis, dim in sides:
        count, length = (lax.axis_size(axis), shard.shape[dim])
        up = [(i, (i + 1) % count) for i in range(count if wrap else count - 1)]
        down = [(j, i) for i, j in up]
        last = lax.slice_in_dim(shard, length - width, length, axis=dim)
        leading = lax.slice_in_dim(shard, 0, width, axis=dim)
        before = lax.ppermute(last, axis, up)
        after = lax.ppermute(leading, axis, down)
        shard = jnp.concatenate([before, shard, after], axis=dim)
    return shard


def rms_rows(stream, gain_row):
    values = stream.astype(jnp.float32)
    mean_sq = jnp.mean(values * values, axis=-1, keepdims=True)
    return (values * lax.rsqrt(mean_sq + EPS) * gain_row).astype(jnp.bfloat16)


def head_norm(heads_raw):
    values = heads_raw.astype(jnp.float32)
    mean_sq = jnp.mean(values * values, axis=-1, keepdims=True)
    return (values * lax.rsqrt(mean_sq + EPS)).astype(jnp.bfloat16)


def attend(queries, fringe, seg_own, seg_fringe, bias_layer):
    row_count, grid_width, head_count, head_width = queries.shape
    key_rows = jnp.stack(
        [fringe[row_lag : row_lag + row_count] for row_lag in range(WIN_ROWS)], axis=1
    )
    seg_rows = jnp.stack(
        [seg_fringe[row_lag : row_lag + row_count] for row_lag in range(WIN_ROWS)], axis=1
    )
    key_part = key_rows[..., :head_width]
    value_part = key_rows[..., head_width:]
    scores = jnp.einsum(
        "rchd,rjkhd->rhcjk", queries, key_part, preferred_element_type=jnp.float32
    ) * head_width ** (-0.5)
    column = jnp.arange(grid_width)
    col_offset = column[None, :] - column[:, None] + WIN_COLS // 2
    inside = (col_offset >= 0) & (col_offset < WIN_COLS)
    bias_table = bias_layer[:, :, jnp.clip(col_offset, 0, WIN_COLS - 1)]
    scores = scores + jnp.transpose(bias_table, (0, 2, 1, 3))[None]
    same_doc = seg_rows[:, None, None, :, :] == seg_own[:, None, :, None, None]
    allowed = same_doc & inside[None, None, :, None, :]
    scores = jnp.where(allowed, scores, -1e30)
    flat = scores.reshape(row_count, head_count, grid_width, WIN_ROWS * grid_width)
    attn_probs = jax.nn.softmax(flat, axis=-1).astype(jnp.bfloat16)
    attn_probs = attn_probs.reshape(row_count, head_count, grid_width, WIN_ROWS, grid_width)
    mixed_heads = jnp.einsum(
        "rhcjk,rjkhd->rchd", attn_probs, value_part, preferred_element_type=jnp.float32
    )
    return mixed_heads.astype(jnp.bfloat16)


def body(tokens, norm_gain, w_query, w_key, w_value, w_out, offset_bias, documents):
    token_count = tokens.shape[0]
    row_count = token_count // GRID_W
    reach_rows = WIN_ROWS // 2
    head_count = offset_bias.shape[1]
    seg_own = (documents + 1).reshape(row_count, GRID_W)
    seg_fringe = with_halo(seg_own, (("sp", 0),), reach_rows, False)
    collected = (
        lax.all_gather(w_query, "sp", axis=1, tiled=True),
        lax.all_gather(w_key, "sp", axis=1, tiled=True),
        lax.all_gather(w_value, "sp", axis=1, tiled=True),
        lax.all_gather(w_out, "sp", axis=2, tiled=True),
    )
    stream = tokens
    for layer_index in range(LAYERS):
        gathered = lax.all_gather(stream, "tp", axis=1, tiled=True)
        normed = rms_rows(gathered, norm_gain[layer_index])
        query_raw = jnp.dot(normed, collected[0][layer_index], preferred_element_type=jnp.float32)
        key_raw = jnp.dot(normed, collected[1][layer_index], preferred_element_type=jnp.float32)
        value_raw = jnp.dot(normed, collected[2][layer_index], preferred_element_type=jnp.float32)
        query_heads = head_norm(
            query_raw.astype(jnp.bfloat16).reshape(row_count, GRID_W, head_count, HEAD_DIM)
        )
        key_heads = head_norm(
            key_raw.astype(jnp.bfloat16).reshape(row_count, GRID_W, head_count, HEAD_DIM)
        )
        value_heads = value_raw.astype(jnp.bfloat16).reshape(
            row_count, GRID_W, head_count, HEAD_DIM
        )
        key_value = jnp.concatenate([key_heads, value_heads], axis=-1)
        fringe = with_halo(key_value, (("sp", 0),), reach_rows, False)
        attended = attend(query_heads, fringe, seg_own, seg_fringe, offset_bias[layer_index])
        attended = attended.reshape(token_count, head_count * HEAD_DIM)
        partial_sums = jnp.dot(
            attended, collected[3][layer_index], preferred_element_type=jnp.float32
        )
        stream = (
            lax.psum_scatter(
                partial_sums.astype(jnp.bfloat16), "tp", scatter_dimension=1, tiled=True
            )
            .astype(jnp.float32)
            .astype(jnp.bfloat16)
        )
    return stream


def solution(mesh):
    return jax.shard_map(
        body,
        mesh=mesh,
        in_specs=(
            P("sp", "tp"),
            P(),
            P(None, "sp", "tp"),
            P(None, "sp", "tp"),
            P(None, "sp", "tp"),
            P(None, "tp", "sp"),
            P(None, "tp", None, None),
            P("sp"),
        ),
        out_specs=P("sp", "tp"),
        check_vma=False,
    )
```

profile of v0, /device:TPU:0, one launch (start us, length us, event | category | flops | bytes accessed | tf_op | source)
XLA Modules:
  0.0 309.1 jit_solution(167499018848324964)
XLA Ops:
  6.5 0.7 all-gather.5.cloned.1.call-update
  7.3 0.7 all-gather.7.cloned.1.call-update
  8.1 0.7 all-gather.9.cloned.1.call-update
  9.5 4.9 %collective-permute-start.2 = (s32[4,32]{1,0:T(4,128)S(1)}, s32[4,32]{1,0:T(4,128)S(1)}, u32[]{:S(2)}, u32[]{:S(2)}) collective-permute-start(s32[4,32]{1,0:T(4,128)S(1)} %reshape.186), channel_id=1, source_target_pairs={{0,4},{4,8},{8,12},{12,16},{16,20},{20,24},{24,28},{1,5},{5,9},{9,... | collective-permute-start | bytes 1544 | tf_op jit(solution)/shard_map/ppermute | solution.py:21
  14.4 1.3 collective-permute-start.3
  15.8 6.0 %all_gather.21 = bf16[128,1024]{1,0:T(8,128)(2,1)S(1)} all-gather(bf16[128,256]{1,0:T(8,128)(2,1)} %param.8), channel_id=1, replica_groups=mesh['sp'=8,'tp'=4] {'tp'}, dimensions={1}, use_global_device_ids=true | all-gather | bytes 327680 | tf_op jit(solution)/shard_map/all_gather | solution.py:84
  21.9 0.8 fusion.79
  22.8 0.8 fusion.78
  23.8 3.5 %gather_fusion = f32[1024,4,8]{2,1,0:T(4,128)S(1)} fusion(f32[4,8,16]{1,0,2:T(4,128)S(1)} %bitcast.251, s32[1024]{0:T(1024)S(1)} %broadcast_clamp_fusion), kind=kCustom, calls=%fused_computation | custom fusion | bytes 266240 | tf_op jit(solution)/shard_map/gather | solution.py:55
  27.3 1.3 copy.150
  29.0 27.4 %all-gather.5.cloned.1.call-done = bf16[3,1024,256]{2,1,0:T(8,128)(2,1)} async-done(((bf16[3,128,256]{2,1,0:T(8,128)(2,1)}), bf16[3,1024,256]{2,1,0:T(8,128)(2,1)}) %all-gather.5.cloned.1.call-update) | async-done | bytes 1572880 | tf_op jit(solution)/shard_map/all_gather | solution.py:78
  56.4 1.3 fusion.17
  58.4 42.8 %all-gather.7.cloned.1.call-done = bf16[3,1024,256]{2,1,0:T(8,128)(2,1)} async-done(((bf16[3,128,256]{2,1,0:T(8,128)(2,1)}), bf16[3,1024,256]{2,1,0:T(8,128)(2,1)}) %all-gather.7.cloned.1.call-update) | async-done | bytes 1572880 | tf_op jit(solution)/shard_map/all_gather | solution.py:79
  101.2 1.3 convolution_convert_fusion.10
  102.8 2.5 collective-permute-start
  105.2 1.3 collective-permute-start.1
  106.5 39.4 %all-gather.9.cloned.1.call-done = bf16[3,1024,256]{2,1,0:T(8,128)(2,1)} async-done(((bf16[3,128,256]{2,1,0:T(8,128)(2,1)}), bf16[3,1024,256]{2,1,0:T(8,128)(2,1)}) %all-gather.9.cloned.1.call-update) | async-done | bytes 1572880 | tf_op jit(solution)/shard_map/all_gather | solution.py:77
  146.0 1.3 fusion.16
  148.3 0.7 fusion.3
  149.5 1.1 fusion.11
  150.8 39.8 %all-gather.11.cloned.1.call-done = bf16[3,256,1024]{2,1,0:T(8,128)(2,1)} async-done(((bf16[3,256,128]{2,1,0:T(8,128)(2,1)}), bf16[3,256,1024]{2,1,0:T(8,128)(2,1)}) %all-gather.11.cloned.1.call-update) | async-done | bytes 1572880 | tf_op jit(solution)/shard_map/all_gather | solution.py:80
  190.7 2.0 convolution_convert_fusion.2
  192.8 3.6 %gather_fusion.1 = f32[1024,4,8]{2,1,0:T(4,128)S(1)} fusion(f32[4,8,16]{1,0,2:T(4,128)S(1)} %bitcast.252, s32[1024]{0:T(1024)S(1)} %broadcast_clamp_fusion), kind=kCustom, calls=%fused_computation.1 | custom fusion | bytes 266240 | tf_op jit(solution)/shard_map/gather | solution.py:55
  196.4 1.3 copy.167
  197.6 13.6 %reduce-scatter.4.cloned.1.call-done = bf16[128,256]{1,0:T(8,128)(2,1)} async-done(((bf16[128,1024]{1,0:T(8,128)(2,1)}), bf16[128,256]{1,0:T(8,128)(2,1)}) %reduce-scatter.4.cloned.1.call-update) | async-done | bytes 65552 | tf_op jit(solution)/shard_map/reduce_scatter | solution.py:106
  211.2 6.0 %all_gather.26 = bf16[128,1024]{1,0:T(8,128)(2,1)S(1)} all-gather(bf16[128,256]{1,0:T(8,128)(2,1)} %reduce-scatter.4.cloned.1.call-done), channel_id=1, replica_groups=mesh['sp'=8,'tp'=4] {'tp'}, dimensions={1}, use_global_device_ids=true | all-gather | bytes 327680 | tf_op jit(solution)/shard_map/all_gather | solution.py:84
  217.4 1.3 fusion.15
  219.3 1.3 convolution_convert_fusion.7
  220.9 3.4 %collective-permute-start.4 = (bf16[4,32,4,128]{3,1,2,0:T(8,128)(2,1)S(1)}, bf16[4,32,4,128]{3,1,2,0:T(8,128)(2,1)S(1)}, u32[]{:S(2)}, u32[]{:S(2)}) collective-permute-start(bf16[4,32,4,128]{3,1,2,0:T(8,128)(2,1)S(1)} %pad_maximum_fusion.4), channel_id=1, source_target_pairs={{0,4},{4,8},{8,12},{12,16},{16,20},{20,24},{24,28},{1,5},{5,9},{9,... | collective-permute-start | bytes 393224 | tf_op jit(solution)/shard_map/ppermute | solution.py:21
  224.3 1.5 collective-permute-start.5
  225.8 1.3 fusion.14
  227.7 3.9 %collective-permute-done.5 = bf16[4,32,4,128]{3,1,2,0:T(8,128)(2,1)S(1)} collective-permute-done((bf16[4,32,4,128]{3,1,2,0:T(8,128)(2,1)S(1)}, bf16[4,32,4,128]{3,1,2,0:T(8,128)(2,1)S(1)}, u32[]{:S(2)}, u32[]{:S(2)}) %collective-permute-start.5) | collective-permute-done | bytes 131104 | tf_op jit(solution)/shard_map/ppermute | solution.py:22
  232.0 0.7 fusion.4
  233.3 1.1 fusion.10
  234.6 2.0 convolution_convert_fusion.1
  236.7 3.5 %gather_fusion.2 = f32[1024,4,8]{2,1,0:T(4,128)S(1)} fusion(f32[4,8,16]{1,0,2:T(4,128)S(1)} %bitcast.250, s32[1024]{0:T(1024)S(1)} %broadcast_clamp_fusion), kind=kCustom, calls=%fused_computation.2 | custom fusion | bytes 266240 | tf_op jit(solution)/shard_map/gather | solution.py:55
  240.3 1.3 copy.184
  241.5 15.2 %reduce-scatter.6.cloned.1.call-done = bf16[128,256]{1,0:T(8,128)(2,1)} async-done(((bf16[128,1024]{1,0:T(8,128)(2,1)}), bf16[128,256]{1,0:T(8,128)(2,1)}) %reduce-scatter.6.cloned.1.call-update) | async-done | bytes 65552 | tf_op jit(solution)/shard_map/reduce_scatter | solution.py:106
  256.7 6.0 %all_gather.27 = bf16[128,1024]{1,0:T(8,128)(2,1)S(1)} all-gather(bf16[128,256]{1,0:T(8,128)(2,1)} %reduce-scatter.6.cloned.1.call-done), channel_id=1, replica_groups=mesh['sp'=8,'tp'=4] {'tp'}, dimensions={1}, use_global_device_ids=true | all-gather | bytes 327680 | tf_op jit(solution)/shard_map/all_gather | solution.py:84
  262.9 1.3 fusion.13
  264.8 1.3 convolution_convert_fusion.4
  266.4 3.4 %collective-permute-start.6 = (bf16[4,32,4,128]{3,1,2,0:T(8,128)(2,1)S(1)}, bf16[4,32,4,128]{3,1,2,0:T(8,128)(2,1)S(1)}, u32[]{:S(2)}, u32[]{:S(2)}) collective-permute-start(bf16[4,32,4,128]{3,1,2,0:T(8,128)(2,1)S(1)} %pad_maximum_fusion.5), channel_id=1, source_target_pairs={{0,4},{4,8},{8,12},{12,16},{16,20},{20,24},{24,28},{1,5},{5,9},{9,... | collective-permute-start | bytes 393224 | tf_op jit(solution)/shard_map/ppermute | solution.py:21
  269.8 1.3 collective-permute-start.7
  271.1 1.3 fusion.12
  273.1 4.1 %collective-permute-done.7 = bf16[4,32,4,128]{3,1,2,0:T(8,128)(2,1)S(1)} collective-permute-done((bf16[4,32,4,128]{3,1,2,0:T(8,128)(2,1)S(1)}, bf16[4,32,4,128]{3,1,2,0:T(8,128)(2,1)S(1)}, u32[]{:S(2)}, u32[]{:S(2)}) %collective-permute-start.7) | collective-permute-done | bytes 131104 | tf_op jit(solution)/shard_map/ppermute | solution.py:22
  278.8 1.1 fusion.9
  280.1 2.0 convolution_convert_fusion
  282.1 20.2 %reduce-scatter.8.cloned.1.call-done = bf16[128,256]{1,0:T(8,128)(2,1)} async-done(((bf16[128,1024]{1,0:T(8,128)(2,1)}), bf16[128,256]{1,0:T(8,128)(2,1)}) %reduce-scatter.8.cloned.1.call-update) | async-done | bytes 65552 | tf_op jit(solution)/shard_map/reduce_scatter | solution.py:106
  (117 shorter events, 10.6 us)
Async XLA Ops:
  6.5 49.9 %all-gather.5.cloned.1.call-start = ((), (), s32[]{:S(2)}) async-start(), calls=%async_computation.3 | async-start | bytes 1769472 | tf_op jit(solution)/shard_map/all_gather | solution.py:78
  7.3 93.9 %all-gather.7.cloned.1.call-start = ((), (), s32[]{:S(2)}) async-start(), calls=%async_computation.4 | async-start | bytes 1769472 | tf_op jit(solution)/shard_map/all_gather | solution.py:79
  8.0 137.9 %all-gather.9.cloned.1.call-start = ((), (), s32[]{:S(2)}) async-start(), calls=%async_computation.5 | async-start | bytes 1769472 | tf_op jit(solution)/shard_map/all_gather | solution.py:77
  8.7 181.9 %all-gather.11.cloned.1.call-start = ((), (), s32[]{:S(2)}) async-start(), calls=%async_computation.6 | async-start | bytes 1769472 | tf_op jit(solution)/shard_map/all_gather | solution.py:80
  9.5 19.1 %collective-permute-start.2 = (s32[4,32]{1,0:T(4,128)S(1)}, s32[4,32]{1,0:T(4,128)S(1)}, u32[]{:S(2)}, u32[]{:S(2)}) collective-permute-start(s32[4,32]{1,0:T(4,128)S(1)} %reshape.186), channel_id=1, source_target_pairs={{0,4},{4,8},{8,12},{12,16},{16,20},{20,24},{24,28},{1,5},{5,9},{9,... | collective-permute-start | bytes 1544 | tf_op jit(solution)/shard_map/ppermute | solution.py:21
  14.4 14.2 %collective-permute-start.3 = (s32[4,32]{1,0:T(4,128)S(1)}, s32[4,32]{1,0:T(4,128)S(1)}, u32[]{:S(2)}, u32[]{:S(2)}) collective-permute-start(s32[4,32]{1,0:T(4,128)S(1)} %reshape.186), channel_id=1, source_target_pairs={{4,0},{8,4},{12,8},{16,12},{20,16},{24,20},{28,24},{5,1},{9,5},{13... | collective-permute-start | bytes 1544 | tf_op jit(solution)/shard_map/ppermute | solution.py:22
  15.7 195.5 %reduce-scatter.4.cloned.1.call-start = ((), (), s32[]{:S(2)}) async-start(), calls=%async_computation.7 | async-start | bytes 327680 | tf_op jit(solution)/shard_map/reduce_scatter | solution.py:106
  102.8 45.1 %collective-permute-start = (bf16[4,32,4,128]{3,1,2,0:T(8,128)(2,1)S(1)}, bf16[4,32,4,128]{3,1,2,0:T(8,128)(2,1)S(1)}, u32[]{:S(2)}, u32[]{:S(2)}) collective-permute-start(bf16[4,32,4,128]{3,1,2,0:T(8,128)(2,1)S(1)} %pad_maximum_fusion.3), channel_id=1, source_target_pairs={{0,4},{4,8},{8,12},{12,16},{16,20},{20,24},{24,28},{1,5},{5,9},{9,... | collective-permute-start | bytes 393224 | tf_op jit(solution)/shard_map/ppermute | solution.py:21
  105.2 42.7 %collective-permute-start.1 = (bf16[4,32,4,128]{3,1,2,0:T(8,128)(2,1)S(1)}, bf16[4,32,4,128]{3,1,2,0:T(8,128)(2,1)S(1)}, u32[]{:S(2)}, u32[]{:S(2)}) collective-permute-start(bf16[4,32,4,128]{3,1,2,0:T(8,128)(2,1)S(1)} %pad_maximum_fusion.3), channel_id=1, source_target_pairs={{4,0},{8,4},{12,8},{16,12},{20,16},{24,20},{28,24},{5,1},{9,5},{13... | collective-permute-start | bytes 393224 | tf_op jit(solution)/shard_map/ppermute | solution.py:22
  192.7 64.1 %reduce-scatter.6.cloned.1.call-start = ((), (), s32[]{:S(2)}) async-start(), calls=%async_computation.8 | async-start | bytes 327680 | tf_op jit(solution)/shard_map/reduce_scatter | solution.py:106
  220.9 6.8 %collective-permute-start.4 = (bf16[4,32,4,128]{3,1,2,0:T(8,128)(2,1)S(1)}, bf16[4,32,4,128]{3,1,2,0:T(8,128)(2,1)S(1)}, u32[]{:S(2)}, u32[]{:S(2)}) collective-permute-start(bf16[4,32,4,128]{3,1,2,0:T(8,128)(2,1)S(1)} %pad_maximum_fusion.4), channel_id=1, source_target_pairs={{0,4},{4,8},{8,12},{12,16},{16,20},{20,24},{24,28},{1,5},{5,9},{9,... | collective-permute-start | bytes 393224 | tf_op jit(solution)/shard_map/ppermute | solution.py:21
  224.3 7.4 %collective-permute-start.5 = (bf16[4,32,4,128]{3,1,2,0:T(8,128)(2,1)S(1)}, bf16[4,32,4,128]{3,1,2,0:T(8,128)(2,1)S(1)}, u32[]{:S(2)}, u32[]{:S(2)}) collective-permute-start(bf16[4,32,4,128]{3,1,2,0:T(8,128)(2,1)S(1)} %pad_maximum_fusion.4), channel_id=1, source_target_pairs={{4,0},{8,4},{12,8},{16,12},{20,16},{24,20},{28,24},{5,1},{9,5},{13... | collective-permute-start | bytes 393224 | tf_op jit(solution)/shard_map/ppermute | solution.py:22
  236.6 65.7 %reduce-scatter.8.cloned.1.call-start = ((), (), s32[]{:S(2)}) async-start(), calls=%async_computation.9 | async-start | bytes 327680 | tf_op jit(solution)/shard_map/reduce_scatter | solution.py:106
  266.4 6.6 %collective-permute-start.6 = (bf16[4,32,4,128]{3,1,2,0:T(8,128)(2,1)S(1)}, bf16[4,32,4,128]{3,1,2,0:T(8,128)(2,1)S(1)}, u32[]{:S(2)}, u32[]{:S(2)}) collective-permute-start(bf16[4,32,4,128]{3,1,2,0:T(8,128)(2,1)S(1)} %pad_maximum_fusion.5), channel_id=1, source_target_pairs={{0,4},{4,8},{8,12},{12,16},{16,20},{20,24},{24,28},{1,5},{5,9},{9,... | collective-permute-start | bytes 393224 | tf_op jit(solution)/shard_map/ppermute | solution.py:21
  269.8 7.4 %collective-permute-start.7 = (bf16[4,32,4,128]{3,1,2,0:T(8,128)(2,1)S(1)}, bf16[4,32,4,128]{3,1,2,0:T(8,128)(2,1)S(1)}, u32[]{:S(2)}, u32[]{:S(2)}) collective-permute-start(bf16[4,32,4,128]{3,1,2,0:T(8,128)(2,1)S(1)} %pad_maximum_fusion.5), channel_id=1, source_target_pairs={{4,0},{8,4},{12,8},{16,12},{20,16},{24,20},{28,24},{5,1},{9,5},{13... | collective-permute-start | bytes 393224 | tf_op jit(solution)/shard_map/ppermute | solution.py:22
Sparse Core Ops, SparseCore 0:
  9.5 46.8 all-gather.4
  58.6 42.5 all-gather.6
  103.4 42.5 all-gather.8
  147.8 42.7 all-gather.10
  193.0 18.2 reduce-scatter.3
  236.7 19.9 reduce-scatter.5
  282.2 20.0 reduce-scatter.7
where the time goes:
time: 310 us; the launch traced here: 309 us
  waiting for transfers between devices  209 us (67%)
  matrix products  23 us (7%)
  starting transfers between devices  19.7 us (6%)
  local copies, waits for them, and re-layouts  19.3 us (6%)
  blocking collectives  17.9 us (6%)
  between operations  14.2 us (5%)
  other arithmetic  6.3 us (2%)
    reduce_scatter x3, waiting for transfers between devices, body(): lax.psum_scatter(partial_sums.astype(jnp.bfloat16), 'tp', scatter_dimensi...  49 us
    all_gather x1, waiting for transfers between devices, body(): lax.all_gather(w_value, 'sp', axis=1, tiled=True)  42.8 us
    all_gather x1, waiting for transfers between devices, body(): lax.all_gather(w_out, 'sp', axis=2, tiled=True)  39.8 us
    all_gather x1, waiting for transfers between devices, body(): lax.all_gather(w_query, 'sp', axis=1, tiled=True)  39.4 us
    all_gather x1, waiting for transfers between devices, body(): lax.all_gather(w_key, 'sp', axis=1, tiled=True)  27.4 us
    all_gather x3, blocking collectives, body(): gathered = lax.all_gather(stream, 'tp', axis=1, tiled=True)  17.9 us
    gather x6, local copies, waits for them, and re-layouts, attend(): bias_table = bias_layer[:, :, jnp.clip(col_offset, 0, WIN_COLS - 1)]  14.4 us
    ppermute x4, starting transfers between devices, with_halo(): before = lax.ppermute(last, axis, up)  14.1 us
  transfers between devices with their start and end apart: 15, of which 9 were waited for; matrix products, arithmetic and copies ran while one was open for 10% of the time, Pallas kernels for 0%

commit v1 on v0

--- a/solution.py
+++ b/solution.py
@@ -9,6 +9,27 @@
 LAYERS = 3
 GRID_W = 32
 EPS = 1e-06
+
+
+def joined_along(tiles, dim):
+    dims = list(tiles.shape[1:])
+    dims[dim] *= tiles.shape[0]
+    return jnp.moveaxis(tiles, 0, dim).reshape(dims)
+
+
+def collected_by_bits(x, axis):
+    size, here = (lax.axis_size(axis), lax.axis_index(axis))
+    parts, bit = (x[None], 1)
+    while bit < size:
+        received = lax.ppermute(parts, axis, [(i, i ^ bit) for i in range(size)])
+        low = here & bit == 0
+        parts = jnp.concatenate([jnp.where(low, parts, received), jnp.where(low, received, parts)])
+        bit *= 2
+    return parts
+
+
+def doubled_up(x, axis, dim):
+    return joined_along(collected_by_bits(x, axis), dim)
 
 
 def with_halo(shard, sides, width, wrap):
@@ -81,7 +102,7 @@
     )
     stream = tokens
     for layer_index in range(LAYERS):
-        gathered = lax.all_gather(stream, "tp", axis=1, tiled=True)
+        gathered = doubled_up(stream, "tp", 1)
         normed = rms_rows(gathered, norm_gain[layer_index])
         query_raw = jnp.dot(normed, collected[0][layer_index], preferred_element_type=jnp.float32)
         key_raw = jnp.dot(normed, collected[1][layer_index], preferred_element_type=jnp.float32)

time: 310 us -> 316 us (1.019)
  waiting for transfers between devices: 209 us -> 227 us
  blocking collectives: 17.9 us -> 0 us
    all_gather x3 -> x0, blocking collectives: 17.9 us -> none  [body(): gathered = lax.all_gather(stream, 'tp', axis=1, tiled=True)]
    reduce_scatter x3, waiting for transfers between devices: 49 us -> 60.6 us  [body(): lax.psum_scatter(partial_sums.astype(jnp.bfloat16), 'tp', scatter_dimensi...]
    ppermute x0 -> x6, waiting for transfers between devices: none -> 7.84 us  [collected_by_bits(): received = lax.ppermute(parts, axis, [(i, i ^ bit) for i in range(size)])]
  transfers between devices with their start and end apart: 15 -> 21, of which waited for: 9 -> 14; matrix products, arithmetic and copies ran while one was open for 10% -> 10% of each run, Pallas kernels for 0% -> 0%
where the time goes in v1:
time: 316 us; the launch traced here: 315 us
  waiting for transfers between devices  227 us (72%)
  matrix products  22.9 us (7%)
  starting transfers between devices  22 us (7%)
  local copies, waits for them, and re-layouts  19.9 us (6%)
  between operations  14.3 us (5%)
  other arithmetic  8.58 us (3%)
    reduce_scatter x3, waiting for transfers between devices, body(): lax.psum_scatter(partial_sums.astype(jnp.bfloat16), 'tp', scatter_dimensi...  60.6 us
    all_gather x1, waiting for transfers between devices, body(): lax.all_gather(w_value, 'sp', axis=1, tiled=True)  42.8 us
    all_gather x1, waiting for transfers between devices, body(): lax.all_gather(w_out, 'sp', axis=2, tiled=True)  39.8 us
    all_gather x1, waiting for transfers between devices, body(): lax.all_gather(w_query, 'sp', axis=1, tiled=True)  39.4 us
    all_gather x1, waiting for transfers between devices, body(): lax.all_gather(w_key, 'sp', axis=1, tiled=True)  27.2 us
    gather x6, local copies, waits for them, and re-layouts, attend(): bias_table = bias_layer[:, :, jnp.clip(col_offset, 0, WIN_COLS - 1)]  14.4 us
    ppermute x4, starting transfers between devices, with_halo(): before = lax.ppermute(last, axis, up)  14.1 us
    ppermute x6, waiting for transfers between devices, collected_by_bits(): received = lax.ppermute(parts, axis, [(i, i ^ bit) for i in range(size)])  7.84 us
  transfers between devices with their start and end apart: 21, of which 14 were waited for; matrix products, arithmetic and copies ran while one was open for 10% of the time, Pallas kernels for 0%

profile of v1, /device:TPU:0, one launch (start us, length us, event | category | flops | bytes accessed | tf_op | source)
XLA Modules:
  0.0 314.6 jit_solution(18083222385793629556)
XLA Ops:
  6.5 0.7 all-gather.5.cloned.1.call-update
  7.3 0.7 all-gather.7.cloned.1.call-update
  9.5 4.9 %collective-permute-start.4 = (s32[4,32]{1,0:T(4,128)S(1)}, s32[4,32]{1,0:T(4,128)S(1)}, u32[]{:S(2)}, u32[]{:S(2)}) collective-permute-start(s32[4,32]{1,0:T(4,128)S(1)} %reshape.288), channel_id=1, source_target_pairs={{0,4},{4,8},{8,12},{12,16},{16,20},{20,24},{24,28},{1,5},{5,9},{9,... | collective-permute-start | bytes 1544 | tf_op jit(solution)/shard_map/ppermute | solution.py:42
  14.4 1.3 collective-permute-start.5
  16.0 0.9 slice_reduce_fusion.2
  16.9 0.8 fusion.72
  17.8 3.6 %gather_fusion = f32[1024,4,8]{2,1,0:T(4,128)S(1)} fusion(f32[4,8,16]{1,0,2:T(4,128)S(1)} %bitcast.275, s32[1024]{0:T(1024)S(1)} %broadcast_clamp_fusion), kind=kCustom, calls=%fused_computation | custom fusion | bytes 266240 | tf_op jit(solution)/shard_map/gather | solution.py:76
  21.3 1.3 copy.157
  22.8 1.6 collective-permute-start.1
  24.6 4.2 %collective-permute-done.1 = bf16[2,128,256]{2,1,0:T(8,128)(2,1)S(1)} collective-permute-done((bf16[2,128,256]{2,1,0:T(8,128)(2,1)S(1)}, bf16[2,128,256]{2,1,0:T(8,128)(2,1)S(1)}, u32[]{:S(2)}, u32[]{:S(2)}) %collective-permute-start.1) | collective-permute-done | bytes 131104 | tf_op jit(solution)/shard_map/ppermute | solution.py:24
  29.3 27.2 %all-gather.5.cloned.1.call-done = bf16[3,1024,256]{2,1,0:T(8,128)(2,1)} async-done(((bf16[3,128,256]{2,1,0:T(8,128)(2,1)}), bf16[3,1024,256]{2,1,0:T(8,128)(2,1)}) %all-gather.5.cloned.1.call-update) | async-done | bytes 1572880 | tf_op jit(solution)/shard_map/all_gather | solution.py:99
  56.5 1.3 fusion.17
  58.4 42.8 %all-gather.7.cloned.1.call-done = bf16[3,1024,256]{2,1,0:T(8,128)(2,1)} async-done(((bf16[3,128,256]{2,1,0:T(8,128)(2,1)}), bf16[3,1024,256]{2,1,0:T(8,128)(2,1)}) %all-gather.7.cloned.1.call-update) | async-done | bytes 1572880 | tf_op jit(solution)/shard_map/all_gather | solution.py:100
  101.3 1.3 convolution_convert_fusion.10
  102.8 2.5 collective-permute-start.2
  105.3 1.3 collective-permute-start.3
  106.6 39.4 %all-gather.9.cloned.1.call-done = bf16[3,1024,256]{2,1,0:T(8,128)(2,1)} async-done(((bf16[3,128,256]{2,1,0:T(8,128)(2,1)}), bf16[3,1024,256]{2,1,0:T(8,128)(2,1)}) %all-gather.9.cloned.1.call-update) | async-done | bytes 1572880 | tf_op jit(solution)/shard_map/all_gather | solution.py:98
  146.0 1.3 fusion.16
  149.6 1.1 fusion.11
  150.9 39.8 %all-gather.11.cloned.1.call-done = bf16[3,256,1024]{2,1,0:T(8,128)(2,1)} async-done(((bf16[3,256,128]{2,1,0:T(8,128)(2,1)}), bf16[3,256,1024]{2,1,0:T(8,128)(2,1)}) %all-gather.11.cloned.1.call-update) | async-done | bytes 1572880 | tf_op jit(solution)/shard_map/all_gather | solution.py:101
  190.7 2.0 convolution_convert_fusion.2
  192.8 18.5 %reduce-scatter.4.cloned.1.call-done = bf16[128,256]{1,0:T(8,128)(2,1)} async-done(((bf16[128,1024]{1,0:T(8,128)(2,1)}), bf16[128,256]{1,0:T(8,128)(2,1)}) %reduce-scatter.4.cloned.1.call-update) | async-done | bytes 65552 | tf_op jit(solution)/shard_map/reduce_scatter | solution.py:127
  211.3 1.5 collective-permute-done.6
  212.8 0.9 broadcast_select_fusion.9
  214.1 3.6 %gather_fusion.1 = f32[1024,4,8]{2,1,0:T(4,128)S(1)} fusion(f32[4,8,16]{1,0,2:T(4,128)S(1)} %bitcast.276, s32[1024]{0:T(1024)S(1)} %broadcast_clamp_fusion), kind=kCustom, calls=%fused_computation.1 | custom fusion | bytes 266240 | tf_op jit(solution)/shard_map/gather | solution.py:76
  217.7 1.3 copy.175
  219.8 1.3 fusion.15
  221.7 1.3 convolution_convert_fusion.7
  223.3 3.4 %collective-permute-start.8 = (bf16[4,32,4,128]{3,1,2,0:T(8,128)(2,1)S(1)}, bf16[4,32,4,128]{3,1,2,0:T(8,128)(2,1)S(1)}, u32[]{:S(2)}, u32[]{:S(2)}) collective-permute-start(bf16[4,32,4,128]{3,1,2,0:T(8,128)(2,1)S(1)} %pad_maximum_fusion.9), channel_id=1, source_target_pairs={{0,4},{4,8},{8,12},{12,16},{16,20},{20,24},{24,28},{1,5},{5,9},{9,... | collective-permute-start | bytes 393224 | tf_op jit(solution)/shard_map/ppermute | solution.py:42
  226.7 1.5 collective-permute-start.9
  228.2 1.3 fusion.14
  230.1 3.4 %collective-permute-done.9 = bf16[4,32,4,128]{3,1,2,0:T(8,128)(2,1)S(1)} collective-permute-done((bf16[4,32,4,128]{3,1,2,0:T(8,128)(2,1)S(1)}, bf16[4,32,4,128]{3,1,2,0:T(8,128)(2,1)S(1)}, u32[]{:S(2)}, u32[]{:S(2)}) %collective-permute-start.9) | collective-permute-done | bytes 131104 | tf_op jit(solution)/shard_map/ppermute | solution.py:43
  235.2 1.1 fusion.10
  236.5 2.0 convolution_convert_fusion.1
  238.5 21.0 %reduce-scatter.6.cloned.1.call-done = bf16[128,256]{1,0:T(8,128)(2,1)} async-done(((bf16[128,1024]{1,0:T(8,128)(2,1)}), bf16[128,256]{1,0:T(8,128)(2,1)}) %reduce-scatter.6.cloned.1.call-update) | async-done | bytes 65552 | tf_op jit(solution)/shard_map/reduce_scatter | solution.py:127
  259.5 1.5 collective-permute-done.10
  261.0 0.9 broadcast_select_fusion.7
  262.3 3.6 %gather_fusion.2 = f32[1024,4,8]{2,1,0:T(4,128)S(1)} fusion(f32[4,8,16]{1,0,2:T(4,128)S(1)} %bitcast.274, s32[1024]{0:T(1024)S(1)} %broadcast_clamp_fusion), kind=kCustom, calls=%fused_computation.2 | custom fusion | bytes 266240 | tf_op jit(solution)/shard_map/gather | solution.py:76
  265.9 1.3 copy.193
  268.0 1.3 fusion.13
  269.9 1.3 convolution_convert_fusion.4
  271.5 3.4 %collective-permute-start.12 = (bf16[4,32,4,128]{3,1,2,0:T(8,128)(2,1)S(1)}, bf16[4,32,4,128]{3,1,2,0:T(8,128)(2,1)S(1)}, u32[]{:S(2)}, u32[]{:S(2)}) collective-permute-start(bf16[4,32,4,128]{3,1,2,0:T(8,128)(2,1)S(1)} %pad_maximum_fusion.11), channel_id=1, source_target_pairs={{0,4},{4,8},{8,12},{12,16},{16,20},{20,24},{24,28},{1,5},{5,9},{9,... | collective-permute-start | bytes 393224 | tf_op jit(solution)/shard_map/ppermute | solution.py:42
  274.9 1.3 collective-permute-start.13
  276.2 1.3 fusion.12
  278.2 3.6 %collective-permute-done.13 = bf16[4,32,4,128]{3,1,2,0:T(8,128)(2,1)S(1)} collective-permute-done((bf16[4,32,4,128]{3,1,2,0:T(8,128)(2,1)S(1)}, bf16[4,32,4,128]{3,1,2,0:T(8,128)(2,1)S(1)}, u32[]{:S(2)}, u32[]{:S(2)}) %collective-permute-start.13) | collective-permute-done | bytes 131104 | tf_op jit(solution)/shard_map/ppermute | solution.py:43
  283.4 1.1 fusion.9
  284.7 2.0 convolution_convert_fusion
  286.7 21.0 %reduce-scatter.8.cloned.1.call-done = bf16[128,256]{1,0:T(8,128)(2,1)} async-done(((bf16[128,1024]{1,0:T(8,128)(2,1)}), bf16[128,256]{1,0:T(8,128)(2,1)}) %reduce-scatter.8.cloned.1.call-update) | async-done | bytes 65552 | tf_op jit(solution)/shard_map/reduce_scatter | solution.py:127
  (146 shorter events, 15.1 us)
Async XLA Ops:
  6.5 50.0 %all-gather.5.cloned.1.call-start = ((), (), s32[]{:S(2)}) async-start(), calls=%async_computation.3 | async-start | bytes 1769472 | tf_op jit(solution)/shard_map/all_gather | solution.py:99
  7.3 94.0 %all-gather.7.cloned.1.call-start = ((), (), s32[]{:S(2)}) async-start(), calls=%async_computation.4 | async-start | bytes 1769472 | tf_op jit(solution)/shard_map/all_gather | solution.py:100
  8.0 138.0 %all-gather.9.cloned.1.call-start = ((), (), s32[]{:S(2)}) async-start(), calls=%async_computation.5 | async-start | bytes 1769472 | tf_op jit(solution)/shard_map/all_gather | solution.py:98
  8.7 182.0 %all-gather.11.cloned.1.call-start = ((), (), s32[]{:S(2)}) async-start(), calls=%async_computation.6 | async-start | bytes 1769472 | tf_op jit(solution)/shard_map/all_gather | solution.py:101
  9.5 13.1 %collective-permute-start.4 = (s32[4,32]{1,0:T(4,128)S(1)}, s32[4,32]{1,0:T(4,128)S(1)}, u32[]{:S(2)}, u32[]{:S(2)}) collective-permute-start(s32[4,32]{1,0:T(4,128)S(1)} %reshape.288), channel_id=1, source_target_pairs={{0,4},{4,8},{8,12},{12,16},{16,20},{20,24},{24,28},{1,5},{5,9},{9,... | collective-permute-start | bytes 1544 | tf_op jit(solution)/shard_map/ppermute | solution.py:42
  14.4 8.2 %collective-permute-start.5 = (s32[4,32]{1,0:T(4,128)S(1)}, s32[4,32]{1,0:T(4,128)S(1)}, u32[]{:S(2)}, u32[]{:S(2)}) collective-permute-start(s32[4,32]{1,0:T(4,128)S(1)} %reshape.288), channel_id=1, source_target_pairs={{4,0},{8,4},{12,8},{16,12},{20,16},{24,20},{28,24},{5,1},{9,5},{13... | collective-permute-start | bytes 1544 | tf_op jit(solution)/shard_map/ppermute | solution.py:43
  15.7 7.1 %copy-start = (bf16[128,256]{1,0:T(8,128)(2,1)S(1)}, bf16[128,256]{1,0:T(8,128)(2,1)}, u32[]{:S(2)}) copy-start(bf16[128,256]{1,0:T(8,128)(2,1)} %param.8) | copy-start | bytes 196612
  15.7 7.0 %collective-permute-start = (bf16[1,128,256]{2,1,0:T(8,128)(2,1)}, bf16[1,128,256]{2,1,0:T(8,128)(2,1)S(1)}, u32[]{:S(2)}, u32[]{:S(2)}) collective-permute-start(bf16[1,128,256]{2,1,0:T(8,128)(2,1)} %bitcast.301), channel_id=1, source_target_pairs={{0,1},{1,0},{2,3},{3,2},{4,5},{5,4},{6,7},{7,6},{8,9},{9,8},{10,11... | collective-permute-start | bytes 196616 | tf_op jit(solution)/shard_map/ppermute | solution.py:24
  15.8 195.5 %reduce-scatter.4.cloned.1.call-start = ((), (), s32[]{:S(2)}) async-start(), calls=%async_computation.7 | async-start | bytes 327680 | tf_op jit(solution)/shard_map/reduce_scatter | solution.py:127
  22.8 6.0 %collective-permute-start.1 = (bf16[2,128,256]{2,1,0:T(8,128)(2,1)S(1)}, bf16[2,128,256]{2,1,0:T(8,128)(2,1)S(1)}, u32[]{:S(2)}, u32[]{:S(2)}) collective-permute-start(bf16[2,128,256]{2,1,0:T(8,128)(2,1)S(1)} %pad_maximum_fusion.6), channel_id=1, source_target_pairs={{0,2},{1,3},{2,0},{3,1},{4,6},{5,7},{6,4},{7,5},{8,10},{9,11},{10,... | collective-permute-start | bytes 393224 | tf_op jit(solution)/shard_map/ppermute | solution.py:24
  102.8 45.1 %collective-permute-start.2 = (bf16[4,32,4,128]{3,1,2,0:T(8,128)(2,1)S(1)}, bf16[4,32,4,128]{3,1,2,0:T(8,128)(2,1)S(1)}, u32[]{:S(2)}, u32[]{:S(2)}) collective-permute-start(bf16[4,32,4,128]{3,1,2,0:T(8,128)(2,1)S(1)} %pad_maximum_fusion.7), channel_id=1, source_target_pairs={{0,4},{4,8},{8,12},{12,16},{16,20},{20,24},{24,28},{1,5},{5,9},{9,... | collective-permute-start | bytes 393224 | tf_op jit(solution)/shard_map/ppermute | solution.py:42
  105.3 42.7 %collective-permute-start.3 = (bf16[4,32,4,128]{3,1,2,0:T(8,128)(2,1)S(1)}, bf16[4,32,4,128]{3,1,2,0:T(8,128)(2,1)S(1)}, u32[]{:S(2)}, u32[]{:S(2)}) collective-permute-start(bf16[4,32,4,128]{3,1,2,0:T(8,128)(2,1)S(1)} %pad_maximum_fusion.7), channel_id=1, source_target_pairs={{4,0},{8,4},{12,8},{16,12},{20,16},{24,20},{28,24},{5,1},{9,5},{13... | collective-permute-start | bytes 393224 | tf_op jit(solution)/shard_map/ppermute | solution.py:43
  192.8 66.8 %reduce-scatter.6.cloned.1.call-start = ((), (), s32[]{:S(2)}) async-start(), calls=%async_computation.8 | async-start | bytes 327680 | tf_op jit(solution)/shard_map/reduce_scatter | solution.py:127
  211.3 1.5 collective-permute-start.6
  213.7 5.6 %collective-permute-start.7 = (bf16[2,128,256]{2,1,0:T(8,128)(2,1)S(1)}, bf16[2,128,256]{2,1,0:T(8,128)(2,1)S(1)}, u32[]{:S(2)}, u32[]{:S(2)}) collective-permute-start(bf16[2,128,256]{2,1,0:T(8,128)(2,1)S(1)} %pad_maximum_fusion.8), channel_id=1, source_target_pairs={{0,2},{1,3},{2,0},{3,1},{4,6},{5,7},{6,4},{7,5},{8,10},{9,11},{10,... | collective-permute-start | bytes 393224 | tf_op jit(solution)/shard_map/ppermute | solution.py:24
  223.3 6.8 %collective-permute-start.8 = (bf16[4,32,4,128]{3,1,2,0:T(8,128)(2,1)S(1)}, bf16[4,32,4,128]{3,1,2,0:T(8,128)(2,1)S(1)}, u32[]{:S(2)}, u32[]{:S(2)}) collective-permute-start(bf16[4,32,4,128]{3,1,2,0:T(8,128)(2,1)S(1)} %pad_maximum_fusion.9), channel_id=1, source_target_pairs={{0,4},{4,8},{8,12},{12,16},{16,20},{20,24},{24,28},{1,5},{5,9},{9,... | collective-permute-start | bytes 393224 | tf_op jit(solution)/shard_map/ppermute | solution.py:42
  226.7 6.9 %collective-permute-start.9 = (bf16[4,32,4,128]{3,1,2,0:T(8,128)(2,1)S(1)}, bf16[4,32,4,128]{3,1,2,0:T(8,128)(2,1)S(1)}, u32[]{:S(2)}, u32[]{:S(2)}) collective-permute-start(bf16[4,32,4,128]{3,1,2,0:T(8,128)(2,1)S(1)} %pad_maximum_fusion.9), channel_id=1, source_target_pairs={{4,0},{8,4},{12,8},{16,12},{20,16},{24,20},{28,24},{5,1},{9,5},{13... | collective-permute-start | bytes 393224 | tf_op jit(solution)/shard_map/ppermute | solution.py:43
  238.5 69.3 %reduce-scatter.8.cloned.1.call-start = ((), (), s32[]{:S(2)}) async-start(), calls=%async_computation.9 | async-start | bytes 327680 | tf_op jit(solution)/shard_map/reduce_scatter | solution.py:127
  259.5 1.5 collective-permute-start.10
  261.9 5.6 %collective-permute-start.11 = (bf16[2,128,256]{2,1,0:T(8,128)(2,1)S(1)}, bf16[2,128,256]{2,1,0:T(8,128)(2,1)S(1)}, u32[]{:S(2)}, u32[]{:S(2)}) collective-permute-start(bf16[2,128,256]{2,1,0:T(8,128)(2,1)S(1)} %pad_maximum_fusion.10), channel_id=1, source_target_pairs={{0,2},{1,3},{2,0},{3,1},{4,6},{5,7},{6,4},{7,5},{8,10},{9,11},{10,... | collective-permute-start | bytes 393224 | tf_op jit(solution)/shard_map/ppermute | solution.py:24
  271.5 6.6 %collective-permute-start.12 = (bf16[4,32,4,128]{3,1,2,0:T(8,128)(2,1)S(1)}, bf16[4,32,4,128]{3,1,2,0:T(8,128)(2,1)S(1)}, u32[]{:S(2)}, u32[]{:S(2)}) collective-permute-start(bf16[4,32,4,128]{3,1,2,0:T(8,128)(2,1)S(1)} %pad_maximum_fusion.11), channel_id=1, source_target_pairs={{0,4},{4,8},{8,12},{12,16},{16,20},{20,24},{24,28},{1,5},{5,9},{9,... | collective-permute-start | bytes 393224 | tf_op jit(solution)/shard_map/ppermute | solution.py:42
  274.9 6.9 %collective-permute-start.13 = (bf16[4,32,4,128]{3,1,2,0:T(8,128)(2,1)S(1)}, bf16[4,32,4,128]{3,1,2,0:T(8,128)(2,1)S(1)}, u32[]{:S(2)}, u32[]{:S(2)}) collective-permute-start(bf16[4,32,4,128]{3,1,2,0:T(8,128)(2,1)S(1)} %pad_maximum_fusion.11), channel_id=1, source_target_pairs={{4,0},{8,4},{12,8},{16,12},{20,16},{24,20},{28,24},{5,1},{9,5},{13... | collective-permute-start | bytes 393224 | tf_op jit(solution)/shard_map/ppermute | solution.py:43
Sparse Core Ops, SparseCore 0:
  9.5 46.9 all-gather.4
  58.7 42.5 all-gather.6
  103.4 42.5 all-gather.8
  147.9 42.7 all-gather.10
  193.0 18.2 reduce-scatter.3
  238.6 20.8 reduce-scatter.5
  286.8 20.8 reduce-scatter.7
